TPU v7x, 512 devices: a whole 4x4x16 slice. The times are simulated.
512 devices in a mesh: tp: 64 (over z, y), dp: 8 (over x, core).
Axes of the slice: x: 4, y: 4, z: 16, core: 2. Of those that a mesh axis runs over, the one named last changes fastest.
Arguments:
- resid: bfloat16 [256, 2048], P('dp', 'tp'), may hold values from -6 to 6
- norm_gain: float32 [2, 2048], replicated, may hold values from 0.1 to 1.9
- w_query: bfloat16 [2, 2048, 2048], P(None, 'dp', 'tp'), may hold values from -0.125 to 0.125
- w_forget: bfloat16 [2, 2048, 2048], P(None, 'dp', 'tp'), may hold values from -0.125 to 0.125
- w_value: bfloat16 [2, 2048, 16, 128], P(None, 'dp', None, 'tp'), may hold values from -0.125 to 0.125
- w_gate: bfloat16 [2, 2048, 16, 128], P(None, 'dp', None, 'tp'), may hold values from -0.125 to 0.125
- gate_floor: float32 [2, 2048], replicated, may hold values from 0 to 0.9
- states: float32 [2, 256, 16, 128, 128], P(None, 'dp', None, 'tp'), may hold values from -1 to 1
- out_gain: float32 [2, 16, 128], P(None, None, 'tp'), may hold values from 0.1 to 1.9
- w_out: bfloat16 [2, 16, 128, 2048], P(None, None, 'tp'), may hold values from -0.125 to 0.125
Outputs:
- new_resid: bfloat16 [256, 2048], P('dp', 'tp')
- new_states: float32 [2, 256, 16, 128, 128], P(None, 'dp', None, 'tp')
All inputs are finite; a program needn't handle non-finite values.
Results may differ from a plain program's by a relative error of at most 0.029.
Values may be sent and summed in bfloat16 or wider, within the bound.
A program may use at most 64 MiB of HBM per device.

v0:
```python
import jax
import jax.numpy as jnp
from jax import lax
from jax.sharding import PartitionSpec as P

BLOCKS = 2
epsilon = 1e-06


def sent_to_all(value, axis):
    length = lax.axis_size(axis)
    return lax.all_to_all(
        jnp.broadcast_to(value[None], (length, *value.shape)), axis, 0, 0, tiled=True
    )


def in_order(parts, dim):
    shape = list(parts.shape[1:])
    shape[dim] *= parts.shape[0]
    return jnp.moveaxis(parts, 0, dim).reshape(shape)


def gather_directly(value, axis, dim):
    parts = sent_to_all(value, axis)
    return in_order(parts, dim)


def in_one_piece(arrays, axis, dim, along):
    ends, at = ([], 0)
    for a in arrays[:-1]:
        at += a.shape[along]
        ends.append(at)
    both = jnp.concatenate(arrays, axis=along)
    return tuple(jnp.split(lax.all_gather(both, axis, axis=dim, tiled=True), ends, axis=along))


def rows_first(arrays, axis, dims):
    turned = [jnp.moveaxis(a, dim, 0) for a, dim in zip(arrays, dims)]
    both = jnp.concatenate([t.reshape(len(t), -1) for t in turned], axis=1)
    out, at, finished = (lax.all_gather(both, axis, axis=0, tiled=True), 0, [])
    for t, dim in zip(turned, dims):
        share = out[:, at : at + t[0].size].reshape(-1, *t.shape[1:])
        finished.append(jnp.moveaxis(share, 0, dim))
        at += t[0].size
    return tuple(finished)


def of_everyone(value, axis):
    everything = sent_to_all(value, axis)
    return jnp.sum(everything, axis=0)


def in_blocks(value, dim, length):
    before, after = (value.shape[:dim], value.shape[dim + 1 :])
    return jnp.moveaxis(value.reshape(*before, length, -1, *after), dim, 0)


def summed_on_arrival(value, axis, dim):
    parts = in_blocks(value, dim, lax.axis_size(axis))
    arrived = lax.all_to_all(parts, axis, split_axis=0, concat_axis=0, tiled=True)
    return arrived.sum(axis=0)


def shards(
    resid, norm_gain, w_query, w_forget, w_value, w_gate, gate_floor, states, out_gain, w_out
):
    residual = resid
    seq_local = resid.shape[0]
    heads = states.shape[2]
    slice_cols = states.shape[3]
    head_dim = states.shape[4]
    row_count = w_query.shape[1]
    new_list = []
    for layer in range(BLOCKS):
        gathered = gather_directly(residual, "tp", 1)
        resid_f32 = gathered.astype(jnp.float32)
        inv_rms = lax.rsqrt(jnp.mean(resid_f32 * resid_f32, axis=1, keepdims=True) + epsilon)
        scaled = (resid_f32 * norm_gain[layer]).astype(jnp.bfloat16)
        query_rows = w_query[layer]
        forget_rows = w_forget[layer]
        value_rows = w_value[layer].reshape(row_count, -1)
        gate_rows = w_gate[layer].reshape(row_count, -1)
        zero_sums = (
            jnp.zeros((seq_local, query_rows.shape[1]), jnp.float32),
            jnp.zeros((seq_local, forget_rows.shape[1]), jnp.float32),
            jnp.zeros((seq_local, value_rows.shape[1]), jnp.float32),
            jnp.zeros((seq_local, gate_rows.shape[1]), jnp.float32),
        )
        totals = zero_sums
        pieces = in_one_piece((query_rows, forget_rows, value_rows, gate_rows), "dp", 0, 1)
        segments = pieces[0].shape[0] // row_count
        for part_index in range(segments):
            columns = lax.dynamic_slice_in_dim(scaled, part_index * row_count, row_count, 1)
            lo_row = part_index * row_count
            totals = tuple(
                (
                    total
                    + lax.optimization_barrier(
                        jnp.dot(
                            columns,
                            segment[lo_row : lo_row + row_count],
                            preferred_element_type=jnp.float32,
                        ).astype(jnp.bfloat16)
                    ).astype(jnp.float32)
                    for total, segment in zip(totals, pieces)
                )
            )
        queries, forget_pre, values, gate_pre = [
            (summed * inv_rms).astype(jnp.bfloat16) for summed in totals
        ]
        query_all, forget_all = rows_first((queries, forget_pre), "tp", (1, 1))
        floor_now = gate_floor[layer]
        keep = floor_now + (1.0 - floor_now) * jax.nn.sigmoid(forget_all.astype(jnp.float32))
        keep = keep.reshape(seq_local, heads, head_dim)
        value_f32 = values.astype(jnp.float32).reshape(seq_local, heads, slice_cols)
        state_new = (
            keep[:, :, None, :] * states[layer]
            + (1.0 - keep)[:, :, None, :] * value_f32[:, :, :, None]
        )
        query_f32 = query_all.astype(jnp.float32).reshape(seq_local, heads, head_dim)
        readout = jnp.sum(query_f32[:, :, None, :] * state_new, axis=3)
        power_sum = of_everyone(jnp.sum(readout * readout, axis=2), "tp")
        mean_square = power_sum[..., None] / head_dim
        gate_f32 = gate_pre.astype(jnp.float32).reshape(seq_local, heads, slice_cols)
        normed = (
            readout * lax.rsqrt(mean_square + epsilon) * out_gain[layer] * jax.nn.silu(gate_f32)
        ).astype(jnp.bfloat16)
        flattened = normed.reshape(seq_local, heads * slice_cols)
        weight_out = w_out[layer].reshape(heads * slice_cols, -1)
        branch = summed_on_arrival(
            lax.dot_general(
                weight_out, flattened, (((0,), (1,)), ((), ())), preferred_element_type=jnp.float32
            ),
            "tp",
            0,
        )
        residual = (residual.astype(jnp.float32) + branch.T).astype(jnp.bfloat16)
        new_list.append(state_new)
    return (residual, jnp.stack(new_list))


def solution(mesh):
    return jax.shard_map(
        shards,
        mesh=mesh,
        in_specs=(
            P("dp", "tp"),
            P(),
            P(None, "dp", "tp"),
            P(None, "dp", "tp"),
            P(None, "dp", None, "tp"),
            P(None, "dp", None, "tp"),
            P(),
            P(None, "dp", None, "tp", None),
            P(None, None, "tp"),
            P(None, None, "tp", None),
        ),
        out_specs=(P("dp", "tp"), P(None, "dp", None, "tp", None)),
        check_vma=False,
    )
```

profile of v0, /device:TPU:2, one launch (start us, length us, event | category | flops | bytes accessed | tf_op | source)
XLA Modules:
  0.0 415.4 jit_solution(12405203772914550517)
XLA Ops:
  0.6 0.8 broadcast_in_dim.8
  1.4 1.1 reshape.98
  2.5 18.9 %all-to-all-start = ((bf16[64,2,512]{2,1,0:T(2,128)(2,1)}), bf16[64,2,512]{2,1,0:T(2,128)(2,1)S(1)}, u32[]{:S(2)}, u32[]{:S(2)}) async-start(bf16[64,2,512]{2,1,0:T(2,128)(2,1)} %reshape.98), calls=%async_computation | async-start | bytes 262144 | tf_op jit(solution)/shard_map/all_to_all | solution.py:12
  22.1 0.6 fusion.165
  22.8 0.7 copy-done.15
  25.6 13.2 %all_gather.12 = bf16[2048,128]{0,1:T(8,128)(2,1)S(1)} all-gather(bf16[256,128]{0,1:T(8,128)(2,1)S(1)} %pad_maximum_fusion.1), channel_id=1, replica_groups=mesh['tp'=64,'dp'=8] {'dp'}, dimensions={0}, use_global_device_ids=true | all-gather | bytes 589824 | tf_op jit(solution)/shard_map/all_gather | solution.py:34
  39.4 0.7 mul.316
  40.1 0.7 copy-done.25
  43.4 0.7 convolution_convert_fusion.39
  44.4 0.7 convolution_convert_fusion.38
  45.4 0.7 convolution_convert_fusion.37
  46.4 0.7 convolution_convert_fusion.36
  47.3 0.7 convolution_convert_fusion.35
  50.8 101.3 %all_gather.13 = bf16[2048,64]{1,0:T(8,128)(2,1)S(1)} all-gather(bf16[32,64]{1,0:T(8,128)(2,1)S(1)} %copy.87), channel_id=1, replica_groups=mesh['tp'=64,'dp'=8] {'tp'}, dimensions={0}, use_global_device_ids=true | all-gather | bytes 266240 | tf_op jit(solution)/shard_map/all_gather | solution.py:40
  153.0 0.7 copy-done.3
  153.9 1.4 fusion.7
  155.5 0.9 reshape.100
  156.4 12.3 %all-to-all-start.1 = ((f32[64,1,512]{2,1,0:T(1,128)}), f32[64,1,512]{2,1,0:T(1,128)S(1)}, u32[]{:S(2)}, u32[]{:S(2)}) async-start(f32[64,1,512]{2,1,0:T(1,128)} %reshape.100), calls=%async_computation.1 | async-start | bytes 262144 | tf_op jit(solution)/shard_map/all_to_all | solution.py:12
  169.1 18.0 %all-to-all-done.1 = f32[64,1,512]{2,1,0:T(1,128)S(1)} async-done(((f32[64,1,512]{2,1,0:T(1,128)}), f32[64,1,512]{2,1,0:T(1,128)S(1)}, u32[]{:S(2)}, u32[]{:S(2)}) %all-to-all-start.1) | async-done | bytes 131104 | tf_op jit(solution)/shard_map/all_to_all | solution.py:12
  187.6 0.9 reduce.4
  191.7 22.7 %all_to_all.30 = f32[64,1,1024]{2,1,0:T(1,128)S(1)} all-to-all(f32[64,1,1024]{2,1,0:T(1,128)S(1)} %reshape.102), channel_id=1, replica_groups=mesh['tp'=64,'dp'=8] {'tp'}, dimensions={0} | all-to-all | bytes 524288 | tf_op jit(solution)/shard_map/all_to_all | solution.py:60
  214.3 1.2 reduce.5
  216.7 1.1 reshape.104
  217.8 4.7 %all-to-all-start.3 = ((bf16[64,2,512]{2,1,0:T(2,128)(2,1)}), bf16[64,2,512]{2,1,0:T(2,128)(2,1)S(1)}, u32[]{:S(2)}, u32[]{:S(2)}) async-start(bf16[64,2,512]{2,1,0:T(2,128)(2,1)} %reshape.104), calls=%async_computation.3 | async-start | bytes 262144 | tf_op jit(solution)/shard_map/all_to_all | solution.py:12
  222.6 0.7 mul.349
  223.3 0.7 copy-done.10
  224.0 0.7 reshape_squeeze.23
  224.8 13.1 %all_gather.14 = bf16[2048,128]{0,1:T(8,128)(2,1)S(1)} all-gather(bf16[256,128]{0,1:T(8,128)(2,1)S(1)} %pad_maximum_fusion.2), channel_id=1, replica_groups=mesh['tp'=64,'dp'=8] {'dp'}, dimensions={0}, use_global_device_ids=true | all-gather | bytes 589824 | tf_op jit(solution)/shard_map/all_gather | solution.py:34
  237.9 0.8 all-to-all-done.3
  244.9 100.7 %all_gather.15 = bf16[2048,64]{1,0:T(8,128)(2,1)S(1)} all-gather(bf16[32,64]{1,0:T(8,128)(2,1)S(1)} %copy.101), channel_id=1, replica_groups=mesh['tp'=64,'dp'=8] {'tp'}, dimensions={0}, use_global_device_ids=true | all-gather | bytes 266240 | tf_op jit(solution)/shard_map/all_gather | solution.py:40
  345.9 1.0 copy.102
  347.8 0.9 copy-done.6
  348.7 1.3 fusion.4
  350.3 0.9 reshape.106
  351.2 12.4 %all-to-all-start.4 = ((f32[64,1,512]{2,1,0:T(1,128)}), f32[64,1,512]{2,1,0:T(1,128)S(1)}, u32[]{:S(2)}, u32[]{:S(2)}) async-start(f32[64,1,512]{2,1,0:T(1,128)} %reshape.106), calls=%async_computation.4 | async-start | bytes 262144 | tf_op jit(solution)/shard_map/all_to_all | solution.py:12
  363.6 0.8 convolution_convert_fusion.2
  364.4 0.8 convolution_convert_fusion.1
  365.2 0.8 convolution_convert_fusion
  366.1 15.6 %all-to-all-done.4 = f32[64,1,512]{2,1,0:T(1,128)S(1)} async-done(((f32[64,1,512]{2,1,0:T(1,128)}), f32[64,1,512]{2,1,0:T(1,128)S(1)}, u32[]{:S(2)}, u32[]{:S(2)}) %all-to-all-start.4) | async-done | bytes 131104 | tf_op jit(solution)/shard_map/all_to_all | solution.py:12
  381.7 0.9 reduce.6
  383.4 0.6 copy-done.7
  384.6 1.6 copy.124
  386.2 2.4 reshape.108
  388.6 5.9 %all-to-all-start.5 = ((f32[64,1,1024]{2,1,0:T(1,128)}), f32[64,1,1024]{2,1,0:T(1,128)S(1)}, u32[]{:S(2)}, u32[]{:S(2)}) async-start(f32[64,1,1024]{2,1,0:T(1,128)} %reshape.108), calls=%async_computation.5 | async-start | bytes 524288 | tf_op jit(solution)/shard_map/all_to_all | solution.py:60
  394.5 1.4 multiply_add_fusion.1
  395.9 1.5 pad_maximum_fusion
  397.4 15.7 %all-to-all-done.5 = f32[64,1,1024]{2,1,0:T(1,128)S(1)} async-done(((f32[64,1,1024]{2,1,0:T(1,128)}), f32[64,1,1024]{2,1,0:T(1,128)S(1)}, u32[]{:S(2)}, u32[]{:S(2)}) %all-to-all-start.5) | async-done | bytes 262176 | tf_op jit(solution)/shard_map/all_to_all | solution.py:60
  413.1 1.2 reduce.7
  (203 shorter events, 26.2 us)
Async XLA Ops:
  1.4 20.0 %copy-start.26 = (f32[2,2048]{1,0:T(2,128)S(1)}, f32[2,2048]{1,0:T(2,128)}, u32[]{:S(2)}) copy-start(f32[2,2048]{1,0:T(2,128)} %param.11) | copy-start | bytes 49156
  2.5 21.7 %copy-start.8 = (bf16[2,16,2,2048]{3,2,1,0:T(2,128)(2,1)S(1)}, bf16[2,16,2,2048]{3,2,1,0:T(2,128)(2,1)}, u32[]{:S(2)}) copy-start(bf16[2,16,2,2048]{3,2,1,0:T(2,128)(2,1)} %param.19) | copy-start | bytes 786436
  2.5 38.9 %all-to-all-start = ((bf16[64,2,512]{2,1,0:T(2,128)(2,1)}), bf16[64,2,512]{2,1,0:T(2,128)(2,1)S(1)}, u32[]{:S(2)}, u32[]{:S(2)}) async-start(bf16[64,2,512]{2,1,0:T(2,128)(2,1)} %reshape.98), calls=%async_computation | async-start | bytes 262144 | tf_op jit(solution)/shard_map/all_to_all | solution.py:12
  21.4 0.8 copy-start.14
  22.8 0.8 copy-start.15
  24.2 0.8 copy-start.18
  24.2 0.8 copy-start.19
  25.6 13.2 %copy-start.30 = (f32[2,16,2]{1,2,0:T(2,128)S(1)}, f32[2,16,2]{1,2,0:T(2,128)}, u32[]{:S(2)}) copy-start(f32[2,16,2]{1,2,0:T(2,128)} %param.18) | copy-start | bytes 772
  40.1 0.7 copy-start.25
  49.8 0.6 copy-start.27
  50.8 102.2 %copy-start.1 = (f32[32,16,2]{2,1,0:T(8,128)}, f32[32,16,2]{2,1,0:T(8,128)S(1)}, u32[]{:S(2)}) copy-start(f32[32,16,2]{2,1,0:T(8,128)S(1)} %copy.91) | copy-start | bytes 12292
  152.6 1.2 copy-start
  153.0 0.7 copy-start.3
  156.4 30.7 %all-to-all-start.1 = ((f32[64,1,512]{2,1,0:T(1,128)}), f32[64,1,512]{2,1,0:T(1,128)S(1)}, u32[]{:S(2)}, u32[]{:S(2)}) async-start(f32[64,1,512]{2,1,0:T(1,128)} %reshape.100), calls=%async_computation.1 | async-start | bytes 262144 | tf_op jit(solution)/shard_map/all_to_all | solution.py:12
  189.0 0.7 copy-start.24
  189.0 0.7 copy-start.28
  189.0 0.7 copy-start.32
  189.2 0.7 copy-start.20
  189.2 0.7 copy-start.21
  189.2 0.7 copy-start.22
  189.2 0.7 copy-start.23
  215.9 0.7 copy-start.13
  216.7 5.8 %copy-start.29 = (f32[1,16,2]{1,2,0:T(2,128)S(1)}, f32[1,16,2]{1,2,0:T(2,128)}, u32[]{:S(2)}) copy-start(f32[1,16,2]{1,2,0:T(2,128)} %get-tuple-element.24) | copy-start | bytes 388
  217.8 20.9 %all-to-all-start.3 = ((bf16[64,2,512]{2,1,0:T(2,128)(2,1)}), bf16[64,2,512]{2,1,0:T(2,128)(2,1)S(1)}, u32[]{:S(2)}, u32[]{:S(2)}) async-start(bf16[64,2,512]{2,1,0:T(2,128)(2,1)} %reshape.104), calls=%async_computation.3 | async-start | bytes 262144 | tf_op jit(solution)/shard_map/all_to_all | solution.py:12
  222.5 0.8 copy-start.9
  223.3 0.7 copy-start.10
  224.0 0.7 copy-start.11
  224.0 0.7 copy-start.12
  237.9 6.4 %copy-start.5 = (bf16[2048,128]{0,1:T(8,128)(2,1)}, bf16[2048,128]{0,1:T(8,128)(2,1)S(1)}, u32[]{:S(2)}) copy-start(bf16[2048,128]{0,1:T(8,128)(2,1)S(1)} %all_gather.14) | copy-start | bytes 1572868
  240.0 0.7 copy-start.17
  346.9 0.7 copy-start.16
  347.7 1.0 copy-start.6
  351.2 30.5 %all-to-all-start.4 = ((f32[64,1,512]{2,1,0:T(1,128)}), f32[64,1,512]{2,1,0:T(1,128)S(1)}, u32[]{:S(2)}, u32[]{:S(2)}) async-start(f32[64,1,512]{2,1,0:T(1,128)} %reshape.106), calls=%async_computation.4 | async-start | bytes 262144 | tf_op jit(solution)/shard_map/all_to_all | solution.py:12
  383.1 0.9 copy-start.7
  383.3 0.7 copy-start.31
  388.6 5.9 %copy-start.2 = (f32[32,16,2]{2,1,0:T(8,128)S(1)}, f32[32,16,2]{2,1,0:T(8,128)}, u32[]{:S(2)}) copy-start(f32[32,16,2]{2,1,0:T(8,128)} %copy-done.1) | copy-start | bytes 12292
  388.6 5.9 %copy-start.4 = (f32[32,16,128]{2,1,0:T(8,128)S(1)}, f32[32,16,128]{2,1,0:T(8,128)}, u32[]{:S(2)}) copy-start(f32[32,16,128]{2,1,0:T(8,128)} %copy-done.3) | copy-start | bytes 786436
  388.6 24.5 %all-to-all-start.5 = ((f32[64,1,1024]{2,1,0:T(1,128)}), f32[64,1,1024]{2,1,0:T(1,128)S(1)}, u32[]{:S(2)}, u32[]{:S(2)}) async-start(f32[64,1,1024]{2,1,0:T(1,128)} %reshape.108), calls=%async_computation.5 | async-start | bytes 524288 | tf_op jit(solution)/shard_map/all_to_all | solution.py:60
where the time goes:
time: 417 us; the launch traced here: 415 us
  blocking collectives  251 us (60%)
  starting transfers between devices  54.2 us (13%)
  waiting for transfers between devices  50 us (12%)
  local copies, waits for them, and re-layouts  31.6 us (8%)
  other arithmetic  13.7 us (3%)
  matrix products  13.7 us (3%)
    all_gather x2, blocking collectives, rows_first(): out, at, finished = (lax.all_gather(both, axis, axis=0, tiled=True), 0, [])  202 us
    all_to_all x4, starting transfers between devices, sent_to_all(): lax.all_to_all(jnp.broadcast_to(value[None], (length, *value.shape)), axi...  48.3 us
    all_to_all x4, waiting for transfers between devices, sent_to_all(): lax.all_to_all(jnp.broadcast_to(value[None], (length, *value.shape)), axi...  34.3 us
    all_gather x2, blocking collectives, in_one_piece(): lax.all_gather(both, axis, axis=dim, tiled=True)  26.3 us
    all_to_all x1, blocking collectives, summed_on_arrival(): lax.all_to_all(parts, axis, split_axis=0, concat_axis=0, tiled=True)  22.7 us
    unnamed x84, local copies, waits for them, and re-layouts  16.5 us
    all_to_all x1, waiting for transfers between devices, summed_on_arrival(): lax.all_to_all(parts, axis, split_axis=0, concat_axis=0, tiled=True)  15.7 us
    dot_general x64, matrix products, shards(): jnp.dot(columns, segment[lo_row:lo_row + row_count], preferred_element_ty...  13.2 us
  transfers between devices with their start and end apart: 5, of which 4 were waited for; matrix products, arithmetic and copies ran while one was open for 3% of the time, Pallas kernels for 0%

commit v1 on v0

--- a/solution.py
+++ b/solution.py
@@ -37,7 +37,13 @@
 def rows_first(arrays, axis, dims):
     turned = [jnp.moveaxis(a, dim, 0) for a, dim in zip(arrays, dims)]
     both = jnp.concatenate([t.reshape(len(t), -1) for t in turned], axis=1)
-    out, at, finished = (lax.all_gather(both, axis, axis=0, tiled=True), 0, [])
+    out, at, finished = (
+        jnp.concatenate(
+            lax.all_to_all(jnp.stack([both] * lax.axis_size(axis)), axis, 0, 0), axis=0
+        ),
+        0,
+        [],
+    )
     for t, dim in zip(turned, dims):
         share = out[:, at : at + t[0].size].reshape(-1, *t.shape[1:])
         finished.append(jnp.moveaxis(share, 0, dim))

time: 417 us -> 278 us (0.67)
  blocking collectives: 251 us -> 52.3 us
  waiting for transfers between devices: 50 us -> 89.6 us
  starting transfers between devices: 54.2 us -> 67.5 us
    all_gather x2 -> x0, blocking collectives: 202 us -> none  [rows_first(): out, at, finished = (lax.all_gather(both, axis, axis=0, tiled=True), 0, [])]
    all_to_all x0 -> x2, waiting for transfers between devices: none -> 38.6 us  [rows_first(): lax.all_to_all(jnp.stack([both] * lax.axis_size(axis)), axis, 0, 0)]
    all_to_all x0 -> x2, starting transfers between devices: none -> 29.2 us  [rows_first(): lax.all_to_all(jnp.stack([both] * lax.axis_size(axis)), axis, 0, 0)]
    all_to_all x4, starting transfers between devices: 48.3 us -> 33.6 us  [sent_to_all(): lax.all_to_all(jnp.broadcast_to(value[None], (length, *value.shape)), axi...]
    unnamed x84 -> x104, local copies, waits for them, and re-layouts: 16.5 us -> 19.9 us
  transfers between devices with their start and end apart: 5 -> 7, of which waited for: 4 -> 6; matrix products, arithmetic and copies ran while one was open for 3% -> 7% of each run, Pallas kernels for 0% -> 0%
where the time goes in v1:
time: 278 us; the launch traced here: 276 us
  waiting for transfers between devices  89.6 us (32%)
  starting transfers between devices  67.5 us (24%)
  blocking collectives  52.3 us (19%)
  local copies, waits for them, and re-layouts  34.4 us (12%)
  matrix products  16.6 us (6%)
  other arithmetic  14.5 us (5%)
    all_to_all x2, waiting for transfers between devices, rows_first(): lax.all_to_all(jnp.stack([both] * lax.axis_size(axis)), axis, 0, 0)  38.6 us
    all_to_all x4, starting transfers between devices, sent_to_all(): lax.all_to_all(jnp.broadcast_to(value[None], (length, *value.shape)), axi...  33.6 us
    all_to_all x4, waiting for transfers between devices, sent_to_all(): lax.all_to_all(jnp.broadcast_to(value[None], (length, *value.shape)), axi...  32.1 us
    all_to_all x2, starting transfers between devices, rows_first(): lax.all_to_all(jnp.stack([both] * lax.axis_size(axis)), axis, 0, 0)  29.2 us
    all_gather x2, blocking collectives, in_one_piece(): lax.all_gather(both, axis, axis=dim, tiled=True)  26.3 us
    all_to_all x1, blocking collectives, summed_on_arrival(): lax.all_to_all(parts, axis, split_axis=0, concat_axis=0, tiled=True)  26 us
    unnamed x104, local copies, waits for them, and re-layouts  19.9 us
    all_to_all x1, waiting for transfers between devices, summed_on_arrival(): lax.all_to_all(parts, axis, split_axis=0, concat_axis=0, tiled=True)  18.8 us
  transfers between devices with their start and end apart: 7, of which 6 were waited for; matrix products, arithmetic and copies ran while one was open for 7% of the time, Pallas kernels for 0%

profile of v1, /device:TPU:2, one launch (start us, length us, event | category | flops | bytes accessed | tf_op | source)
XLA Modules:
  0.0 276.3 jit_solution(3779268150164554865)
XLA Ops:
  0.6 0.8 broadcast_in_dim.8
  1.4 1.1 reshape.110
  2.5 18.9 %all-to-all-start = ((bf16[64,2,512]{2,1,0:T(2,128)(2,1)}), bf16[64,2,512]{2,1,0:T(2,128)(2,1)S(1)}, u32[]{:S(2)}, u32[]{:S(2)}) async-start(bf16[64,2,512]{2,1,0:T(2,128)(2,1)} %reshape.110), calls=%async_computation | async-start | bytes 262144 | tf_op jit(solution)/shard_map/all_to_all | solution.py:12
  22.8 0.7 copy-done.15
  25.6 13.2 %all_gather.6 = bf16[2048,128]{0,1:T(8,128)(2,1)S(1)} all-gather(bf16[256,128]{0,1:T(8,128)(2,1)S(1)} %pad_maximum_fusion.1), channel_id=1, replica_groups=mesh['tp'=64,'dp'=8] {'dp'}, dimensions={0}, use_global_device_ids=true | all-gather | bytes 589824 | tf_op jit(solution)/shard_map/all_gather | solution.py:34
  47.3 1.0 reshape.112
  48.3 15.1 %all-to-all-start.1 = ((bf16[64,2,1024]{2,1,0:T(2,128)(2,1)}), bf16[64,2,1024]{2,1,0:T(2,128)(2,1)S(1)}, u32[]{:S(2)}, u32[]{:S(2)}) async-start(bf16[64,2,1024]{2,1,0:T(2,128)(2,1)} %reshape.112), calls=%async_computation.1 | async-start | bytes 524288 | tf_op jit(solution)/shard_map/all_to_all | solution.py:42
  63.4 0.7 convolution_convert_fusion.39
  64.2 0.7 convolution_convert_fusion.38
  64.9 0.7 convolution_convert_fusion.37
  65.6 0.7 convolution_convert_fusion.36
  66.3 0.7 convolution_convert_fusion.35
  67.0 19.4 %all-to-all-done.1 = bf16[64,2,1024]{2,1,0:T(2,128)(2,1)S(1)} async-done(((bf16[64,2,1024]{2,1,0:T(2,128)(2,1)}), bf16[64,2,1024]{2,1,0:T(2,128)(2,1)S(1)}, u32[]{:S(2)}, u32[]{:S(2)}) %all-to-all-start.1) | async-done | bytes 262176 | tf_op jit(solution)/shard_map/all_to_all | solution.py:42
  89.0 1.4 fusion.7
  90.6 0.9 reshape.114
  91.5 5.1 %all-to-all-start.2 = ((f32[64,1,512]{2,1,0:T(1,128)}), f32[64,1,512]{2,1,0:T(1,128)S(1)}, u32[]{:S(2)}, u32[]{:S(2)}) async-start(f32[64,1,512]{2,1,0:T(1,128)} %reshape.114), calls=%async_computation.2 | async-start | bytes 262144 | tf_op jit(solution)/shard_map/all_to_all | solution.py:12
  96.9 16.5 %all-to-all-done.2 = f32[64,1,512]{2,1,0:T(1,128)S(1)} async-done(((f32[64,1,512]{2,1,0:T(1,128)}), f32[64,1,512]{2,1,0:T(1,128)S(1)}, u32[]{:S(2)}, u32[]{:S(2)}) %all-to-all-start.2) | async-done | bytes 131104 | tf_op jit(solution)/shard_map/all_to_all | solution.py:12
  114.0 0.9 reduce.4
  118.0 26.0 %all_to_all.40 = f32[64,1,1024]{2,1,0:T(1,128)S(1)} all-to-all(f32[64,1,1024]{2,1,0:T(1,128)S(1)} %reshape.116), channel_id=1, replica_groups=mesh['tp'=64,'dp'=8] {'tp'}, dimensions={0} | all-to-all | bytes 524288 | tf_op jit(solution)/shard_map/all_to_all | solution.py:66
  144.1 1.2 reduce.5
  146.5 1.1 reshape.118
  147.5 4.8 %all-to-all-start.4 = ((bf16[64,2,512]{2,1,0:T(2,128)(2,1)}), bf16[64,2,512]{2,1,0:T(2,128)(2,1)S(1)}, u32[]{:S(2)}, u32[]{:S(2)}) async-start(bf16[64,2,512]{2,1,0:T(2,128)(2,1)} %reshape.118), calls=%async_computation.4 | async-start | bytes 262144 | tf_op jit(solution)/shard_map/all_to_all | solution.py:12
  154.5 13.1 %all_gather.7 = bf16[2048,128]{0,1:T(8,128)(2,1)S(1)} all-gather(bf16[256,128]{0,1:T(8,128)(2,1)S(1)} %pad_maximum_fusion.2), channel_id=1, replica_groups=mesh['tp'=64,'dp'=8] {'dp'}, dimensions={0}, use_global_device_ids=true | all-gather | bytes 589824 | tf_op jit(solution)/shard_map/all_gather | solution.py:34
  167.6 1.2 all-to-all-done.4
  175.0 1.0 reshape.120
  176.0 14.1 %all-to-all-start.5 = ((bf16[64,2,1024]{2,1,0:T(2,128)(2,1)}), bf16[64,2,1024]{2,1,0:T(2,128)(2,1)S(1)}, u32[]{:S(2)}, u32[]{:S(2)}) async-start(bf16[64,2,1024]{2,1,0:T(2,128)(2,1)} %reshape.120), calls=%async_computation.5 | async-start | bytes 524288 | tf_op jit(solution)/shard_map/all_to_all | solution.py:42
  190.1 0.7 convolution_convert_fusion.7
  190.8 0.7 convolution_convert_fusion.6
  191.6 0.7 convolution_convert_fusion.5
  192.3 0.7 convolution_convert_fusion.4
  193.0 0.7 convolution_convert_fusion.3
  193.7 19.2 %all-to-all-done.5 = bf16[64,2,1024]{2,1,0:T(2,128)(2,1)S(1)} async-done(((bf16[64,2,1024]{2,1,0:T(2,128)(2,1)}), bf16[64,2,1024]{2,1,0:T(2,128)(2,1)S(1)}, u32[]{:S(2)}, u32[]{:S(2)}) %all-to-all-start.5) | async-done | bytes 262176 | tf_op jit(solution)/shard_map/all_to_all | solution.py:42
  213.3 1.0 slice_convert_fusion
  216.2 1.3 fusion.4
  217.8 0.9 reshape.122
  218.7 4.9 %all-to-all-start.6 = ((f32[64,1,512]{2,1,0:T(1,128)}), f32[64,1,512]{2,1,0:T(1,128)S(1)}, u32[]{:S(2)}, u32[]{:S(2)}) async-start(f32[64,1,512]{2,1,0:T(1,128)} %reshape.122), calls=%async_computation.6 | async-start | bytes 262144 | tf_op jit(solution)/shard_map/all_to_all | solution.py:12
  223.6 0.8 convolution_convert_fusion.2
  224.4 0.8 convolution_convert_fusion.1
  225.3 0.8 convolution_convert_fusion
  226.1 14.5 %all-to-all-done.6 = f32[64,1,512]{2,1,0:T(1,128)S(1)} async-done(((f32[64,1,512]{2,1,0:T(1,128)}), f32[64,1,512]{2,1,0:T(1,128)S(1)}, u32[]{:S(2)}, u32[]{:S(2)}) %all-to-all-start.6) | async-done | bytes 131104 | tf_op jit(solution)/shard_map/all_to_all | solution.py:12
  240.6 0.9 reduce.6
  243.6 1.6 copy.136
  245.2 2.4 reshape.124
  247.6 4.7 %all-to-all-start.7 = ((f32[64,1,1024]{2,1,0:T(1,128)}), f32[64,1,1024]{2,1,0:T(1,128)S(1)}, u32[]{:S(2)}, u32[]{:S(2)}) async-start(f32[64,1,1024]{2,1,0:T(1,128)} %reshape.124), calls=%async_computation.7 | async-start | bytes 524288 | tf_op jit(solution)/shard_map/all_to_all | solution.py:66
  252.4 1.4 multiply_add_fusion.1
  253.8 1.5 pad_maximum_fusion
  255.3 18.8 %all-to-all-done.7 = f32[64,1,1024]{2,1,0:T(1,128)S(1)} async-done(((f32[64,1,1024]{2,1,0:T(1,128)}), f32[64,1,1024]{2,1,0:T(1,128)S(1)}, u32[]{:S(2)}, u32[]{:S(2)}) %all-to-all-start.7) | async-done | bytes 262176 | tf_op jit(solution)/shard_map/all_to_all | solution.py:66
  274.0 1.2 reduce.7
  (227 shorter events, 33.4 us)
Async XLA Ops:
  1.4 20.0 %copy-start.32 = (f32[2,2048]{1,0:T(2,128)S(1)}, f32[2,2048]{1,0:T(2,128)}, u32[]{:S(2)}) copy-start(f32[2,2048]{1,0:T(2,128)} %param.11) | copy-start | bytes 49156
  2.5 21.7 %copy-start.8 = (bf16[2,16,2,2048]{3,2,1,0:T(2,128)(2,1)S(1)}, bf16[2,16,2,2048]{3,2,1,0:T(2,128)(2,1)}, u32[]{:S(2)}) copy-start(bf16[2,16,2,2048]{3,2,1,0:T(2,128)(2,1)} %param.19) | copy-start | bytes 786436
  2.5 38.9 %all-to-all-start = ((bf16[64,2,512]{2,1,0:T(2,128)(2,1)}), bf16[64,2,512]{2,1,0:T(2,128)(2,1)S(1)}, u32[]{:S(2)}, u32[]{:S(2)}) async-start(bf16[64,2,512]{2,1,0:T(2,128)(2,1)} %reshape.110), calls=%async_computation | async-start | bytes 262144 | tf_op jit(solution)/shard_map/all_to_all | solution.py:12
  21.4 0.8 copy-start.14
  22.8 0.8 copy-start.15
  24.2 0.8 copy-start.19
  24.2 0.8 copy-start.20
  25.6 13.2 %copy-start.38 = (f32[2,16,2]{1,2,0:T(2,128)S(1)}, f32[2,16,2]{1,2,0:T(2,128)}, u32[]{:S(2)}) copy-start(f32[2,16,2]{1,2,0:T(2,128)} %param.18) | copy-start | bytes 772
  40.1 0.7 copy-start.31
  46.3 0.6 copy-start.33
  47.2 41.0 %copy-start.1 = (f32[32,16,2]{2,1,0:T(8,128)}, f32[32,16,2]{2,1,0:T(8,128)S(1)}, u32[]{:S(2)}) copy-start(f32[32,16,2]{2,1,0:T(8,128)S(1)} %copy.103) | copy-start | bytes 12292
  48.3 38.1 %all-to-all-start.1 = ((bf16[64,2,1024]{2,1,0:T(2,128)(2,1)}), bf16[64,2,1024]{2,1,0:T(2,128)(2,1)S(1)}, u32[]{:S(2)}, u32[]{:S(2)}) async-start(bf16[64,2,1024]{2,1,0:T(2,128)(2,1)} %reshape.112), calls=%async_computation.1 | async-start | bytes 524288 | tf_op jit(solution)/shard_map/all_to_all | solution.py:42
  87.4 0.7 copy-start.18
  87.4 1.6 copy-start
  88.3 0.7 copy-start.3
  91.5 21.9 %all-to-all-start.2 = ((f32[64,1,512]{2,1,0:T(1,128)}), f32[64,1,512]{2,1,0:T(1,128)S(1)}, u32[]{:S(2)}, u32[]{:S(2)}) async-start(f32[64,1,512]{2,1,0:T(1,128)} %reshape.114), calls=%async_computation.2 | async-start | bytes 262144 | tf_op jit(solution)/shard_map/all_to_all | solution.py:12
  115.4 0.7 copy-start.25
  115.4 0.7 copy-start.34
  115.4 0.7 copy-start.40
  115.6 0.7 copy-start.21
  115.6 0.7 copy-start.22
  115.6 0.7 copy-start.23
  115.6 0.7 copy-start.24
  145.7 0.7 copy-start.13
  146.5 5.9 %copy-start.37 = (f32[1,16,2]{1,2,0:T(2,128)S(1)}, f32[1,16,2]{1,2,0:T(2,128)}, u32[]{:S(2)}) copy-start(f32[1,16,2]{1,2,0:T(2,128)} %get-tuple-element.24) | copy-start | bytes 388
  147.5 21.3 %all-to-all-start.4 = ((bf16[64,2,512]{2,1,0:T(2,128)(2,1)}), bf16[64,2,512]{2,1,0:T(2,128)(2,1)S(1)}, u32[]{:S(2)}, u32[]{:S(2)}) async-start(bf16[64,2,512]{2,1,0:T(2,128)(2,1)} %reshape.118), calls=%async_computation.4 | async-start | bytes 262144 | tf_op jit(solution)/shard_map/all_to_all | solution.py:12
  152.3 0.7 copy-start.9
  153.1 0.7 copy-start.10
  153.8 0.7 copy-start.11
  153.8 0.7 copy-start.12
  167.6 25.4 %copy-start.6 = (bf16[2048,128]{0,1:T(8,128)(2,1)}, bf16[2048,128]{0,1:T(8,128)(2,1)S(1)}, u32[]{:S(2)}) copy-start(bf16[2048,128]{0,1:T(8,128)(2,1)S(1)} %all_gather.7) | copy-start | bytes 1572868
  170.1 0.7 copy-start.17
  173.9 0.6 copy-start.35
  176.0 36.9 %all-to-all-start.5 = ((bf16[64,2,1024]{2,1,0:T(2,128)(2,1)}), bf16[64,2,1024]{2,1,0:T(2,128)(2,1)S(1)}, u32[]{:S(2)}, u32[]{:S(2)}) async-start(bf16[64,2,1024]{2,1,0:T(2,128)(2,1)} %reshape.120), calls=%async_computation.5 | async-start | bytes 524288 | tf_op jit(solution)/shard_map/all_to_all | solution.py:42
  214.3 1.0 copy-start.5
  215.3 0.7 copy-start.16
  218.7 21.9 %all-to-all-start.6 = ((f32[64,1,512]{2,1,0:T(1,128)}), f32[64,1,512]{2,1,0:T(1,128)S(1)}, u32[]{:S(2)}, u32[]{:S(2)}) async-start(f32[64,1,512]{2,1,0:T(1,128)} %reshape.122), calls=%async_computation.6 | async-start | bytes 262144 | tf_op jit(solution)/shard_map/all_to_all | solution.py:12
  242.0 0.9 copy-start.7
  242.0 0.9 copy-start.30
  242.1 0.9 copy-start.36
  242.1 0.9 copy-start.39
  242.3 0.7 copy-start.26
  242.3 0.7 copy-start.27
  242.3 0.7 copy-start.28
  242.3 0.8 copy-start.29
  247.6 4.8 %copy-start.2 = (f32[32,16,2]{2,1,0:T(8,128)S(1)}, f32[32,16,2]{2,1,0:T(8,128)}, u32[]{:S(2)}) copy-start(f32[32,16,2]{2,1,0:T(8,128)} %copy-done.1) | copy-start | bytes 12292
  247.6 4.8 %copy-start.4 = (f32[32,16,128]{2,1,0:T(8,128)S(1)}, f32[32,16,128]{2,1,0:T(8,128)}, u32[]{:S(2)}) copy-start(f32[32,16,128]{2,1,0:T(8,128)} %copy-done.3) | copy-start | bytes 786436
  247.6 26.4 %all-to-all-start.7 = ((f32[64,1,1024]{2,1,0:T(1,128)}), f32[64,1,1024]{2,1,0:T(1,128)S(1)}, u32[]{:S(2)}, u32[]{:S(2)}) async-start(f32[64,1,1024]{2,1,0:T(1,128)} %reshape.124), calls=%async_computation.7 | async-start | bytes 524288 | tf_op jit(solution)/shard_map/all_to_all | solution.py:66
